TPU v7x, 32 devices: a whole 2x2x4 slice. The times are simulated.
32 devices in a mesh: gr: 2 (over x), fs: 8 (over z, y), tp: 2 (over core).
Axes of the slice: x: 2, y: 2, z: 4, core: 2. Of those that a mesh axis runs over, the one named last changes fastest.
Arguments:
- prompt: bfloat16 [2048, 2048], P(('gr', 'tp'), 'fs'), may hold values from -2.5 to 2.5
- gain_pre: float32 [2048], P(('gr', 'fs')), may hold values from 0.1 to 1.9
- gate_pre: float32 [2048, 5632], P(('gr', 'fs'), 'tp'), may hold values from -6 to 6
- up_pre: float32 [2048, 5632], P(('gr', 'fs'), 'tp'), may hold values from -6 to 6
- down_pre: float32 [2048, 5632], P(('gr', 'fs'), 'tp'), may hold values from -6 to 6
- gain_post: float32 [2048], P(('gr', 'fs')), may hold values from 0.1 to 1.9
- gate_post: float32 [2048, 5632], P(('gr', 'fs'), 'tp'), may hold values from -6 to 6
- up_post: float32 [2048, 5632], P(('gr', 'fs'), 'tp'), may hold values from -6 to 6
- down_post: float32 [2048, 5632], P(('gr', 'fs'), 'tp'), may hold values from -6 to 6
Outputs:
- result: bfloat16 [2048, 2048], P(('gr', 'tp'), 'fs')
- gate_first: bfloat16 [5632, 2048], P('fs')
- up_first: bfloat16 [5632, 2048], P('fs')
- down_first: bfloat16 [5632, 2048], P('fs')
- gate_second: bfloat16 [5632, 2048], P('fs')
- up_second: bfloat16 [5632, 2048], P('fs')
- down_second: bfloat16 [5632, 2048], P('fs')
All inputs are finite; a program needn't handle non-finite values.
Results may differ from a plain program's by a relative error of at most 0.028.
Values may be sent and summed in bfloat16 or wider, within the bound.
A program may use at most 128 MiB of HBM per device.

v0:
```python
import functools

import jax
import jax.numpy as jnp
from jax import lax
from jax.experimental import pallas as pl
from jax.experimental.pallas import tpu as pltpu
from jax.sharding import PartitionSpec as P

MESH = pl.DeviceIdType.MESH
LANES = 128


def lanes_of(block, width):
    return pl.ds(pl.multiple_of(block * width, width), width)


class HandOver:
    def __init__(self, shards, sources, held, land, first, onward):
        self.n, self.half = shards, shards // 2
        self.sources, self.held = sources, held
        self.land, self.first, self.onward = land, first, onward
        self.g, self.f, self.t = lax.axis_index("gr"), lax.axis_index("fs"), lax.axis_index("tp")
        self.height = held.shape[1]

    def slot(self, m, column):
        return self.held.at[m, :, lanes_of(column, LANES)]

    def copy(self, m, column, source, send, target):
        return pltpu.make_async_remote_copy(
            src_ref=source,
            dst_ref=self.slot(m, column),
            send_sem=send,
            recv_sem=self.land.at[m, column],
            device_id=target,
            device_id_type=MESH,
        )

    def outgoing(self, m, k, act):
        home = lax.rem(self.f, 2)
        target = self.t * self.half + k
        column = self.g * self.n + self.f
        block = self.sources[m].at[pl.ds(k * self.height, self.height), :]
        stays = jnp.logical_and(target == self.f, home == self.t)

        @pl.when(jnp.logical_not(stays))
        def _():
            act(self.copy(m, column, block, self.first.at[m, k], (self.g, target, home)))

        return stays, column, block

    def send(self, m):
        for k in range(self.half):
            stays, column, block = self.outgoing(m, k, lambda c: c.start())

            @pl.when(stays)
            def _():
                pltpu.make_async_copy(block, self.slot(m, column), self.land.at[m, column]).start()

    def arrived(self, m, column):
        slot = self.slot(m, column)
        pltpu.make_async_copy(slot, slot, self.land.at[m, column]).wait()

    def forward(self, m, i, column, which):
        target = (1 - self.g, self.f, self.t) if which == 0 else (self.g, self.f, 1 - self.t)
        return self.copy(m, column, self.slot(m, column), self.onward.at[m, which * self.half + i], target)

    def near(self, i):
        return self.g * self.n + 2 * i + self.t

    def far(self, i):
        return (1 - self.g) * self.n + 2 * i + self.t

    def relay_near(self, m):
        for i in range(self.half):
            self.arrived(m, self.near(i))
            self.forward(m, i, self.near(i), 0).start()
            self.forward(m, i, self.near(i), 1).start()

    def relay_far(self, m):
        for i in range(self.half):
            self.arrived(m, self.far(i))
            self.forward(m, i, self.far(i), 2).start()

    def settle(self, m):
        for group in range(2):
            for i in range(self.half):
                self.arrived(m, group * self.n + 2 * i + 1 - self.t)

    def drain(self, m):
        for k in range(self.half):
            self.outgoing(m, k, lambda c: c.wait_send())
        for i in range(self.half):
            self.forward(m, i, self.near(i), 0).wait_send()
            self.forward(m, i, self.near(i), 1).wait_send()
            self.forward(m, i, self.far(i), 2).wait_send()


def greet(shards):
    g, f, t = lax.axis_index("gr"), lax.axis_index("fs"), lax.axis_index("tp")
    barrier = pltpu.get_barrier_semaphore()
    for step in range(1, 2 * shards):
        place = lax.rem(2 * f + t + step, 2 * shards)
        pl.semaphore_signal(barrier, inc=1, device_id=(g, place // 2, lax.rem(place, 2)), device_id_type=MESH)
    pl.semaphore_signal(barrier, inc=1, device_id=(1 - g, f, t), device_id_type=MESH)
    pl.semaphore_wait(barrier, 2 * shards)


class Tokens:
    def __init__(self, shards, step, x, gathered, gather_out, over_y, into_y, y_out, y_in, over_z, into_z, z_out, z_in):
        self.n, self.depth, self.step = shards, shards // 2, step
        self.x, self.gathered, self.gather_out = x.at[step], gathered, gather_out
        self.over_y, self.into_y, self.y_out, self.y_in = over_y, into_y, y_out, y_in
        self.over_z, self.into_z, self.z_out, self.z_in = over_z, into_z, z_out, z_in
        self.g, self.f, self.t = lax.axis_index("gr"), lax.axis_index("fs"), lax.axis_index("tp")
        self.z, self.y = self.f // 2, lax.rem(self.f, 2)
        self.width = over_y.shape[-1]
        self.sent = []

    def go(self, when, make):
        @pl.when(when)
        def _():
            make().start()

        self.sent.append((when, make))

    def copy(self, source, dest, send, recv, target):
        return pltpu.make_async_remote_copy(
            src_ref=source,
            dst_ref=dest,
            send_sem=send,
            recv_sem=recv,
            device_id=(self.g, target, self.t),
            device_id_type=MESH,
        )

    def piece(self, owner):
        return self.x.at[:, lanes_of(owner, self.width)]

    def hand_on(self, when, source, owner, sem, target):
        self.go(when, lambda: self.copy(source(), self.piece(owner), self.gather_out.at[self.step, sem], self.gathered.at[self.step, owner], target))

    def spread(self, own):
        self.hand_on(self.z < self.depth - 1, lambda: own, self.f, 0, self.f + 2)
        self.hand_on(self.z > 0, lambda: own, self.f, 1, self.f - 2)
        self.hand_on(self.z >= 0, lambda: own, self.f, 2, 2 * self.z + 1 - self.y)

    def came(self, owner):
        piece = self.piece(owner)
        pltpu.make_async_copy(piece, piece, self.gathered.at[self.step, owner]).wait()

    def pass_on(self):
        for i in range(self.depth - 1):
            for side, sign in enumerate((-1, 1)):
                place = self.z + sign * (1 + i)
                owner = 2 * place + self.y
                there = jnp.logical_and(place >= 0, place < self.depth)
                further = jnp.logical_and(there, self.z < self.depth - 1 if sign < 0 else self.z > 0)
                sem = 3 + 4 * i + 2 * side

                @pl.when(there)
                def _(owner=owner):
                    self.came(owner)

                self.hand_on(further, lambda owner=owner: self.piece(owner), owner, sem, self.f - 2 * sign)
                self.hand_on(there, lambda owner=owner: self.piece(owner), owner, sem + 1, 2 * self.z + 1 - self.y)

    def collect(self):
        for i in range(self.depth):
            self.came(2 * i + 1 - self.y)

    def activate(self, w_gate, w_up, hidden, features):
        rows = self.x.shape[0]
        chunk = rows // 2

        @pl.loop(0, 2)
        def _(c):
            span = pl.ds(pl.multiple_of(c * chunk, chunk), chunk)
            tokens = self.x[span, :]
            widened = tokens.astype(jnp.float32)
            squares = jnp.sum(widened * widened, axis=1, keepdims=True)
            scale = lax.rsqrt(squares / features + norm_eps) * features ** (-0.5)
            dims = (((1,), (1,)), ((), ()))
            gate = lax.dot_general(tokens, w_gate[...], dims, preferred_element_type=jnp.float32) * scale
            up = lax.dot_general(tokens, w_up[...], dims, preferred_element_type=jnp.float32) * scale
            hidden[span, :] = (gate / (1.0 + jnp.exp(-gate)) * up).astype(jnp.bfloat16)

    def term(self, hidden, w_down, owner):
        return jnp.dot(hidden[...], w_down[:, lanes_of(owner, self.width)], preferred_element_type=jnp.float32)

    def order(self):
        ends = [(self.depth - 1 - i, i) for i in range(self.depth // 2)]
        return [place for pair in ends for place in pair]

    def reduce_pairs(self, hidden, w_down):
        s = self.step
        for i in self.order():
            self.over_y[s, i] = self.term(hidden, w_down, 2 * i + 1 - self.y).astype(jnp.bfloat16)
            self.go(
                self.z >= 0,
                lambda i=i: self.copy(self.over_y.at[s, i], self.into_y.at[s, i], self.y_out.at[s, i], self.y_in.at[s, i], 2 * self.z + 1 - self.y),
            )

    def reduce_outer(self, hidden, w_down, own):
        s = self.step
        for i in self.order():
            mine = self.term(hidden, w_down, 2 * i + self.y)
            self.wait(self.into_y.at[s, i], self.y_in.at[s, i])
            own[i] = mine + self.into_y[s, i].astype(jnp.float32)
            for side in range(2):
                onward = self.z < i if side == 0 else self.z > i
                inner = self.z > 0 if side == 0 else self.z < self.depth - 1

                @pl.when(jnp.logical_and(onward, inner))
                def _(side=side):
                    self.wait(self.into_z.at[s, side, i], self.z_in.at[s, side, i])
                    own[i] += self.into_z[s, side, i].astype(jnp.float32)

                @pl.when(onward)
                def _():
                    self.over_z[s, i] = own[i].astype(jnp.bfloat16)

                self.go(
                    onward,
                    lambda i=i, side=side: self.copy(
                        self.over_z.at[s, i],
                        self.into_z.at[s, side, i],
                        self.z_out.at[s, i],
                        self.z_in.at[s, side, i],
                        self.f + 2 - 4 * side,
                    ),
                )

    def wait(self, landed, sem):
        pltpu.make_async_copy(landed, landed, sem).wait()

    def finish(self, own, units):
        s = self.step
        for side in range(2):
            inner = self.z > 0 if side == 0 else self.z < self.depth - 1

            @pl.when(inner)
            def _(side=side):
                self.wait(self.into_z.at[s, side, self.z], self.z_in.at[s, side, self.z])
                own[self.z] += self.into_z[s, side, self.z].astype(jnp.float32)

        before = self.x[:, lanes_of(self.f, self.width)].astype(jnp.float32)
        return (before + 0.5 * units ** (-0.5) * own[self.z]).astype(jnp.bfloat16)

    def drain(self):
        for when, make in self.sent:

            @pl.when(when)
            def _(make=make):
                make().wait_send()


def whole_kernel(shards, features, units, *refs):
    prompt, gains, trained, result, outs = refs[0], refs[1:3], refs[3:9], refs[9], refs[10:16]
    held, land, first, onward, written, x, hidden, own, middle, last = refs[16:26]
    traffic, alone, raw, turned, loaded = refs[26:36], refs[36], refs[37], refs[38], refs[39]
    sources = [turned.at[m] for m in range(6)]
    loads = [pltpu.make_async_copy(trained[m], raw.at[m], loaded.at[m]) for m in range(6)]

    def prepare(m):
        loads[m].wait()

        @pl.loop(0, raw.shape[2] // LANES)
        def _(c):
            span = lanes_of(c, LANES)
            block = raw[m, :, span].T
            if m % 3 < 2:
                block = block * gains[m // 3][...]
            turned[m, span, :] = block.astype(jnp.bfloat16)

        moves.send(m)

    moves = HandOver(shards, sources, held, land, first, onward)
    steps = [Tokens(shards, s, x, *traffic) for s in range(2)]
    store = [pltpu.make_async_copy(held.at[m], outs[m], written.at[m]) for m in range(6)]
    for load in loads:
        load.start()
    greet(shards)
    start = pltpu.make_async_copy(prompt, steps[0].piece(steps[0].f), alone.at[0])
    start.start()
    steps[0].spread(prompt)
    for m in range(3):
        prepare(m)
    moves.relay_near(0)
    steps[0].pass_on()
    moves.relay_near(1)
    moves.relay_far(0)
    prepare(3)
    moves.relay_near(2)
    moves.relay_far(1)
    moves.relay_far(2)
    for m in range(3):
        moves.settle(m)
        store[m].start()
    start.wait()
    steps[0].collect()
    steps[0].activate(held.at[0], held.at[1], hidden, features)
    steps[0].reduce_pairs(hidden, held.at[2])
    prepare(4)
    moves.relay_near(3)
    steps[0].reduce_outer(hidden, held.at[2], own)
    prepare(5)
    moves.relay_far(3)
    tokens = steps[0].finish(own, units)
    middle[...] = tokens
    x[1, :, lanes_of(steps[1].f, steps[1].width)] = tokens
    steps[1].spread(middle)
    moves.relay_near(4)
    steps[1].pass_on()
    moves.relay_near(5)
    moves.relay_far(4)
    moves.relay_far(5)
    for m in range(3, 6):
        moves.settle(m)
        store[m].start()
    steps[1].collect()
    steps[1].activate(held.at[3], held.at[4], hidden, features)
    steps[1].reduce_pairs(hidden, held.at[5])
    steps[1].reduce_outer(hidden, held.at[5], own)
    last[...] = steps[1].finish(own, units)
    end = pltpu.make_async_copy(last, result, alone.at[1])
    end.start()
    for m in range(6):
        moves.drain(m)
        store[m].wait()
    for step in steps:
        step.drain()
    end.wait()


def whole(prompt, gains, trained, shards):
    units = trained[0].shape[1] * lax.axis_size("tp")
    height = units // shards
    features = LANES * lax.axis_size("gr") * shards
    rows, width = prompt.shape
    depth = shards // 2
    any_space = pl.BlockSpec(memory_space=pl.ANY)
    return pl.pallas_call(
        functools.partial(whole_kernel, shards, features, units),
        out_shape=[jax.ShapeDtypeStruct(prompt.shape, jnp.bfloat16)] + [jax.ShapeDtypeStruct((height, features), jnp.bfloat16)] * 6,
        in_specs=[any_space] + [pl.BlockSpec(memory_space=pltpu.VMEM)] * 2 + [any_space] * 6,
        out_specs=[any_space] * 7,
        scratch_shapes=[
            pltpu.VMEM((6, height, features), jnp.bfloat16),
            pltpu.SemaphoreType.DMA((6, 2 * shards)),
            pltpu.SemaphoreType.DMA((6, shards // 2)),
            pltpu.SemaphoreType.DMA((6, 3 * shards // 2)),
            pltpu.SemaphoreType.DMA((6,)),
            pltpu.VMEM((2, rows, features), jnp.bfloat16),
            pltpu.VMEM((rows, height), jnp.bfloat16),
            pltpu.VMEM((depth, rows, width), jnp.float32),
            pltpu.VMEM((rows, width), jnp.bfloat16),
            pltpu.VMEM((rows, width), jnp.bfloat16),
            pltpu.SemaphoreType.DMA((2, shards)),
            pltpu.SemaphoreType.DMA((2, 4 * depth)),
            pltpu.VMEM((2, depth, rows, width), jnp.bfloat16),
            pltpu.VMEM((2, depth, rows, width), jnp.bfloat16),
            pltpu.SemaphoreType.DMA((2, depth)),
            pltpu.SemaphoreType.DMA((2, depth)),
            pltpu.VMEM((2, depth, rows, width), jnp.bfloat16),
            pltpu.VMEM((2, 2, depth, rows, width), jnp.bfloat16),
            pltpu.SemaphoreType.DMA((2, depth)),
            pltpu.SemaphoreType.DMA((2, 2, depth)),
            pltpu.SemaphoreType.DMA((2,)),
            pltpu.VMEM((6,) + trained[0].shape, jnp.float32),
            pltpu.VMEM((6, trained[0].shape[1], LANES), jnp.bfloat16),
            pltpu.SemaphoreType.DMA((6,)),
        ],
        compiler_params=pltpu.CompilerParams(collective_id=0, has_side_effects=True, vmem_limit_bytes=60 << 20),
    )(prompt, *gains, *trained)


D = 2048
FF = 5632


norm_eps = 1e-06


def add_products(columns_in, w_gate, w_up):
    widened = columns_in.astype(jnp.float32)
    dims = (((1,), (1,)), ((), ()))
    return (
        lax.dot_general(columns_in, w_gate, dims, preferred_element_type=jnp.float32),
        lax.dot_general(columns_in, w_up, dims, preferred_element_type=jnp.float32),
        jnp.sum(widened * widened, axis=1),
    )


def half_step(tokens, w_gate, w_up, w_down):
    gate_sum, up_sum, squares = add_products(
        lax.all_gather(tokens, "fs", axis=1, tiled=True), w_gate, w_up
    )
    row_scale = (lax.rsqrt(squares / D + norm_eps) * D ** (-0.5))[:, None]
    hidden = (jax.nn.silu(gate_sum * row_scale) * (up_sum * row_scale)).astype(jnp.bfloat16)
    partial_value = jnp.dot(hidden, w_down, preferred_element_type=jnp.float32)
    summed = lax.psum_scatter(
        partial_value.astype(jnp.bfloat16), "fs", scatter_dimension=1, tiled=True
    ).astype(jnp.float32)
    return (tokens.astype(jnp.float32) + 0.5 * FF ** (-0.5) * summed).astype(jnp.bfloat16)


def restore_rows(matrix, groups, shards, lanes):
    row_total, col_total = matrix.shape
    sub_rows = row_total // (groups * shards * lanes)
    shaped = matrix.reshape(groups, lanes, shards, sub_rows, col_total)
    return jnp.transpose(shaped, (0, 2, 1, 3, 4)).reshape(row_total, col_total)


def relayout(matrices):
    crossed = (
        lax.all_to_all(
            lax.all_to_all(matrices[0], "tp", split_axis=0, concat_axis=1, tiled=True),
            "fs",
            split_axis=1,
            concat_axis=0,
            tiled=True,
        ),
        lax.all_to_all(
            lax.all_to_all(matrices[1], "tp", split_axis=0, concat_axis=1, tiled=True),
            "fs",
            split_axis=1,
            concat_axis=0,
            tiled=True,
        ),
        lax.all_to_all(
            lax.all_to_all(matrices[2], "tp", split_axis=0, concat_axis=1, tiled=True),
            "fs",
            split_axis=1,
            concat_axis=0,
            tiled=True,
        ),
        lax.all_to_all(
            lax.all_to_all(matrices[3], "tp", split_axis=0, concat_axis=1, tiled=True),
            "fs",
            split_axis=1,
            concat_axis=0,
            tiled=True,
        ),
        lax.all_to_all(
            lax.all_to_all(matrices[4], "tp", split_axis=0, concat_axis=1, tiled=True),
            "fs",
            split_axis=1,
            concat_axis=0,
            tiled=True,
        ),
        lax.all_to_all(
            lax.all_to_all(matrices[5], "tp", split_axis=0, concat_axis=1, tiled=True),
            "fs",
            split_axis=1,
            concat_axis=0,
            tiled=True,
        ),
    )
    gathered = (
        lax.all_gather(crossed[0], ("gr", "tp"), axis=0, tiled=True),
        lax.all_gather(crossed[1], ("gr", "tp"), axis=0, tiled=True),
        lax.all_gather(crossed[2], ("gr", "tp"), axis=0, tiled=True),
        lax.all_gather(crossed[3], ("gr", "tp"), axis=0, tiled=True),
        lax.all_gather(crossed[4], ("gr", "tp"), axis=0, tiled=True),
        lax.all_gather(crossed[5], ("gr", "tp"), axis=0, tiled=True),
    )
    groups = lax.axis_size("gr")
    shards = lax.axis_size("fs")
    lanes = lax.axis_size("tp")
    return tuple((restore_rows(matrix, groups, shards, lanes).T for matrix in gathered))


def direct_fits(token_shape, shape):
    shards = lax.axis_size("fs")
    units = shape[1] * lax.axis_size("tp")
    whole_rows = shape[0] == LANES and shape[1] % LANES == 0 and units % (16 * shards) == 0
    whole_tokens = token_shape[0] % 32 == 0 and token_shape[1] % LANES == 0
    pairs = shards % 4 == 0 and lax.axis_size("gr") == 2 and lax.axis_size("tp") == 2
    return whole_rows and whole_tokens and pairs


def local(prompt, gain_pre, gate_pre, up_pre, down_pre, gain_post, gate_post, up_post, down_post):
    rounded = (
        (gain_pre[:, None] * gate_pre).astype(jnp.bfloat16),
        (gain_pre[:, None] * up_pre).astype(jnp.bfloat16),
        down_pre.astype(jnp.bfloat16),
        (gain_post[:, None] * gate_post).astype(jnp.bfloat16),
        (gain_post[:, None] * up_post).astype(jnp.bfloat16),
        down_post.astype(jnp.bfloat16),
    )
    if direct_fits(prompt.shape, gate_pre.shape):
        trained = (gate_pre, up_pre, down_pre, gate_post, up_post, down_post)
        gains = (gain_pre[None, :], gain_post[None, :])
        return tuple(whole(prompt, gains, trained, lax.axis_size("fs")))
    served = relayout(rounded)
    middle = half_step(prompt, served[0], served[1], served[2])
    result = half_step(middle, served[3], served[4], served[5])
    return (result, served[0], served[1], served[2], served[3], served[4], served[5])


def solution(mesh):
    placed = (
        P(("gr", "tp"), "fs"),
        P(("gr", "fs")),
        P(("gr", "fs"), "tp"),
        P(("gr", "fs"), "tp"),
        P(("gr", "fs"), "tp"),
        P(("gr", "fs")),
        P(("gr", "fs"), "tp"),
        P(("gr", "fs"), "tp"),
        P(("gr", "fs"), "tp"),
    )
    return jax.shard_map(
        local,
        mesh=mesh,
        in_specs=placed,
        out_specs=(
            P(("gr", "tp"), "fs"),
            P("fs", None),
            P("fs", None),
            P("fs", None),
            P("fs", None),
            P("fs", None),
            P("fs", None),
        ),
        check_vma=False,
    )
```

profile of v0, /device:TPU:0, one launch (start us, length us, event | category | flops | bytes accessed | tf_op | source)
XLA Modules:
  0.0 263.5 jit_solution(2777549099451377271)
XLA Ops:
  0.6 244.2 %shard_map.144 = (bf16[512,256]{1,0:T(8,128)(2,1)}, bf16[704,2048]{1,0:T(8,128)(2,1)}, bf16[704,2048]{1,0:T(8,128)(2,1)}, bf16[704,2048]{1,0:T(8,128)(2,1)}, bf1...) custom-call(bf16[512,256]{1,0:T(8,128)(2,1)} %refs_0_.1, f32[1,128]{1,0:T(1,128)} %bitcast.2, ...), custom_call_target="tpu_custom_call" | custom-call | tf_op jit(solution)/shard_map/pallas_call | solution.py:343
  244.9 1.7 copy.23
  246.5 0.0 copy-start.4
  246.5 3.9 %copy.24 = bf16[704,2048]{1,0:T(8,128)(2,1)} copy(bf16[704,2048]{1,0:T(8,128)(2,1)} %get-tuple-element.15) | data formatting | bytes 5767168
  250.5 0.0 copy-done.4
  250.5 0.0 copy-start.3
  250.5 1.6 copy.25
  252.0 1.3 copy-done.3
  253.3 0.0 copy-start.2
  253.3 1.6 copy.26
  254.9 1.3 copy-done.2
  256.2 0.0 copy-start.1
  256.2 1.6 copy.27
  257.8 1.3 copy-done.1
  259.0 0.0 copy-start
  259.0 1.6 copy.28
  260.6 1.3 copy-done
  261.9 1.6 copy.29
Async XLA Ops:
  246.5 3.9 %copy-start.4 = (bf16[704,2048]{1,0:T(8,128)(2,1)S(1)}, bf16[704,2048]{1,0:T(8,128)(2,1)}, u32[]{:S(2)}) copy-start(bf16[704,2048]{1,0:T(8,128)(2,1)} %get-tuple-element.16) | copy-start | bytes 8650756
  250.5 2.9 %copy-start.3 = (bf16[704,2048]{1,0:T(8,128)(2,1)S(1)}, bf16[704,2048]{1,0:T(8,128)(2,1)}, u32[]{:S(2)}) copy-start(bf16[704,2048]{1,0:T(8,128)(2,1)} %get-tuple-element.17) | copy-start | bytes 8650756
  253.3 2.9 %copy-start.2 = (bf16[704,2048]{1,0:T(8,128)(2,1)S(1)}, bf16[704,2048]{1,0:T(8,128)(2,1)}, u32[]{:S(2)}) copy-start(bf16[704,2048]{1,0:T(8,128)(2,1)} %get-tuple-element.18) | copy-start | bytes 8650756
  256.2 2.9 %copy-start.1 = (bf16[704,2048]{1,0:T(8,128)(2,1)S(1)}, bf16[704,2048]{1,0:T(8,128)(2,1)}, u32[]{:S(2)}) copy-start(bf16[704,2048]{1,0:T(8,128)(2,1)} %get-tuple-element.19) | copy-start | bytes 8650756
  259.0 2.9 %copy-start = (bf16[704,2048]{1,0:T(8,128)(2,1)S(1)}, bf16[704,2048]{1,0:T(8,128)(2,1)}, u32[]{:S(2)}) copy-start(bf16[704,2048]{1,0:T(8,128)(2,1)} %get-tuple-element.20) | copy-start | bytes 8650756
where the time goes:
time: 264 us; the launch traced here: 263 us
  Pallas kernels  244 us (92%)
  local copies, waits for them, and re-layouts  18.6 us (7%)
    pallas_call x1, Pallas kernels, whole(): pl.pallas_call(functools.partial(whole_kernel, shards, features, units),...  244 us
    unnamed x17, local copies, waits for them, and re-layouts  18.6 us

commit v1 on v0

--- a/solution.py
+++ b/solution.py
@@ -21,10 +21,10 @@
         self.sources, self.held = sources, held
         self.land, self.first, self.onward = land, first, onward
         self.g, self.f, self.t = lax.axis_index("gr"), lax.axis_index("fs"), lax.axis_index("tp")
-        self.height = held.shape[1]
+        self.height = held[0].shape[0]
 
     def slot(self, m, column):
-        return self.held.at[m, :, lanes_of(column, LANES)]
+        return self.held[m].at[:, lanes_of(column, LANES)]
 
     def copy(self, m, column, source, send, target):
         return pltpu.make_async_remote_copy(
@@ -49,13 +49,12 @@
 
         return stays, column, block
 
-    def send(self, m):
-        for k in range(self.half):
-            stays, column, block = self.outgoing(m, k, lambda c: c.start())
-
-            @pl.when(stays)
-            def _():
-                pltpu.make_async_copy(block, self.slot(m, column), self.land.at[m, column]).start()
+    def send(self, m, k):
+        stays, column, block = self.outgoing(m, k, lambda c: c.start())
+
+        @pl.when(stays)
+        def _():
+            pltpu.make_async_copy(block, self.slot(m, column), self.land.at[m, column]).start()
 
     def arrived(self, m, column):
         slot = self.slot(m, column)
@@ -71,16 +70,14 @@
     def far(self, i):
         return (1 - self.g) * self.n + 2 * i + self.t
 
-    def relay_near(self, m):
-        for i in range(self.half):
-            self.arrived(m, self.near(i))
-            self.forward(m, i, self.near(i), 0).start()
-            self.forward(m, i, self.near(i), 1).start()
-
-    def relay_far(self, m):
-        for i in range(self.half):
-            self.arrived(m, self.far(i))
-            self.forward(m, i, self.far(i), 2).start()
+    def relay_near(self, m, i):
+        self.arrived(m, self.near(i))
+        self.forward(m, i, self.near(i), 0).start()
+        self.forward(m, i, self.near(i), 1).start()
+
+    def relay_far(self, m, i):
+        self.arrived(m, self.far(i))
+        self.forward(m, i, self.far(i), 2).start()
 
     def settle(self, m):
         for group in range(2):
@@ -103,7 +100,7 @@
         place = lax.rem(2 * f + t + step, 2 * shards)
         pl.semaphore_signal(barrier, inc=1, device_id=(g, place // 2, lax.rem(place, 2)), device_id_type=MESH)
     pl.semaphore_signal(barrier, inc=1, device_id=(1 - g, f, t), device_id_type=MESH)
-    pl.semaphore_wait(barrier, 2 * shards)
+    return lambda: pl.semaphore_wait(barrier, 2 * shards)
 
 
 class Tokens:
@@ -149,21 +146,20 @@
         piece = self.piece(owner)
         pltpu.make_async_copy(piece, piece, self.gathered.at[self.step, owner]).wait()
 
-    def pass_on(self):
-        for i in range(self.depth - 1):
-            for side, sign in enumerate((-1, 1)):
-                place = self.z + sign * (1 + i)
-                owner = 2 * place + self.y
-                there = jnp.logical_and(place >= 0, place < self.depth)
-                further = jnp.logical_and(there, self.z < self.depth - 1 if sign < 0 else self.z > 0)
-                sem = 3 + 4 * i + 2 * side
-
-                @pl.when(there)
-                def _(owner=owner):
-                    self.came(owner)
-
-                self.hand_on(further, lambda owner=owner: self.piece(owner), owner, sem, self.f - 2 * sign)
-                self.hand_on(there, lambda owner=owner: self.piece(owner), owner, sem + 1, 2 * self.z + 1 - self.y)
+    def pass_on(self, i):
+        for side, sign in enumerate((-1, 1)):
+            place = self.z + sign * (1 + i)
+            owner = 2 * place + self.y
+            there = jnp.logical_and(place >= 0, place < self.depth)
+            further = jnp.logical_and(there, self.z < self.depth - 1 if sign < 0 else self.z > 0)
+            sem = 3 + 4 * i + 2 * side
+
+            @pl.when(there)
+            def _(owner=owner):
+                self.came(owner)
+
+            self.hand_on(further, lambda owner=owner: self.piece(owner), owner, sem, self.f - 2 * sign)
+            self.hand_on(there, lambda owner=owner: self.piece(owner), owner, sem + 1, 2 * self.z + 1 - self.y)
 
     def collect(self):
         for i in range(self.depth):
@@ -188,64 +184,74 @@
     def term(self, hidden, w_down, owner):
         return jnp.dot(hidden[...], w_down[:, lanes_of(owner, self.width)], preferred_element_type=jnp.float32)
 
-    def order(self):
-        ends = [(self.depth - 1 - i, i) for i in range(self.depth // 2)]
-        return [place for pair in ends for place in pair]
-
-    def reduce_pairs(self, hidden, w_down):
+    def place(self, k):
+        n = self.depth
+        low = self.z < n // 2
+        z = jnp.where(low, self.z, n - 1 - self.z)
+        lead = n - 1 - 2 * z
+        j = k - lead
+        nearby = z + (1 - 2 * lax.rem(jnp.maximum(j, 0), 2)) * (z - jnp.maximum(j, 0) // 2)
+        found = jnp.where(j < 0, n - 1 - k, nearby)
+        return jnp.where(low, found, n - 1 - found)
+
+    def swap(self, hidden, w_down, k):
         s = self.step
-        for i in self.order():
-            self.over_y[s, i] = self.term(hidden, w_down, 2 * i + 1 - self.y).astype(jnp.bfloat16)
-            self.go(
-                self.z >= 0,
-                lambda i=i: self.copy(self.over_y.at[s, i], self.into_y.at[s, i], self.y_out.at[s, i], self.y_in.at[s, i], 2 * self.z + 1 - self.y),
-            )
-
-    def reduce_outer(self, hidden, w_down, own):
+        self.over_y[s, k] = self.term(hidden, w_down, 2 * self.place(k) + 1 - self.y).astype(jnp.bfloat16)
+        self.go(
+            self.z >= 0,
+            lambda: self.copy(self.over_y.at[s, k], self.into_y.at[s, k], self.y_out.at[s, k], self.y_in.at[s, k], 2 * self.z + 1 - self.y),
+        )
+
+    def gather_term(self, hidden, w_down, own, k):
         s = self.step
-        for i in self.order():
-            mine = self.term(hidden, w_down, 2 * i + self.y)
-            self.wait(self.into_y.at[s, i], self.y_in.at[s, i])
-            own[i] = mine + self.into_y[s, i].astype(jnp.float32)
-            for side in range(2):
-                onward = self.z < i if side == 0 else self.z > i
-                inner = self.z > 0 if side == 0 else self.z < self.depth - 1
-
-                @pl.when(jnp.logical_and(onward, inner))
-                def _(side=side):
-                    self.wait(self.into_z.at[s, side, i], self.z_in.at[s, side, i])
-                    own[i] += self.into_z[s, side, i].astype(jnp.float32)
-
-                @pl.when(onward)
-                def _():
-                    self.over_z[s, i] = own[i].astype(jnp.bfloat16)
-
-                self.go(
-                    onward,
-                    lambda i=i, side=side: self.copy(
-                        self.over_z.at[s, i],
-                        self.into_z.at[s, side, i],
-                        self.z_out.at[s, i],
-                        self.z_in.at[s, side, i],
-                        self.f + 2 - 4 * side,
-                    ),
-                )
+        own[k] = self.term(hidden, w_down, 2 * self.place(k) + self.y)
+
+    def reduce(self, own, k):
+        s = self.step
+        place = self.place(k)
+        up = place > self.z
+        side = jnp.where(up, 0, 1)
+        inner = jnp.where(up, self.z, self.depth - 1 - self.z) > 0
+        self.wait(self.into_y.at[s, k], self.y_in.at[s, k])
+
+        @pl.when(inner)
+        def _():
+            self.wait(self.into_z.at[s, side, place], self.z_in.at[s, side, place])
+            total = own[k] + self.into_y[s, k].astype(jnp.float32) + self.into_z[s, side, place].astype(jnp.float32)
+            self.over_z[s, k] = total.astype(jnp.bfloat16)
+
+        @pl.when(jnp.logical_not(inner))
+        def _():
+            self.over_z[s, k] = (own[k] + self.into_y[s, k].astype(jnp.float32)).astype(jnp.bfloat16)
+
+        self.go(
+            self.z >= 0,
+            lambda: self.copy(
+                self.over_z.at[s, k],
+                self.into_z.at[s, side, place],
+                self.z_out.at[s, k],
+                self.z_in.at[s, side, place],
+                self.f + 2 - 4 * side,
+            ),
+        )
 
     def wait(self, landed, sem):
         pltpu.make_async_copy(landed, landed, sem).wait()
 
     def finish(self, own, units):
-        s = self.step
+        s, k = self.step, self.depth - 1
+        self.wait(self.into_y.at[s, k], self.y_in.at[s, k])
+        own[k] += self.into_y[s, k].astype(jnp.float32)
         for side in range(2):
             inner = self.z > 0 if side == 0 else self.z < self.depth - 1
 
             @pl.when(inner)
             def _(side=side):
                 self.wait(self.into_z.at[s, side, self.z], self.z_in.at[s, side, self.z])
-                own[self.z] += self.into_z[s, side, self.z].astype(jnp.float32)
+                own[k] += self.into_z[s, side, self.z].astype(jnp.float32)
 
         before = self.x[:, lanes_of(self.f, self.width)].astype(jnp.float32)
-        return (before + 0.5 * units ** (-0.5) * own[self.z]).astype(jnp.bfloat16)
+        return (before + 0.5 * units ** (-0.5) * own[k]).astype(jnp.bfloat16)
 
     def drain(self):
         for when, make in self.sent:
@@ -256,81 +262,115 @@
 
 
 def whole_kernel(shards, features, units, *refs):
-    prompt, gains, trained, result, outs = refs[0], refs[1:3], refs[3:9], refs[9], refs[10:16]
-    held, land, first, onward, written, x, hidden, own, middle, last = refs[16:26]
-    traffic, alone, raw, turned, loaded = refs[26:36], refs[36], refs[37], refs[38], refs[39]
+    prompt, gains, trained, result, held = refs[0], refs[1:3], refs[3:9], refs[9], refs[10:16]
+    land, first, onward, x, hidden, own, middle = refs[16:23]
+    traffic, alone, raw, turned, loaded = refs[23:33], refs[33], refs[34], refs[35], refs[36]
     sources = [turned.at[m] for m in range(6)]
     loads = [pltpu.make_async_copy(trained[m], raw.at[m], loaded.at[m]) for m in range(6)]
+    moves = HandOver(shards, sources, held, land, first, onward)
+    steps = [Tokens(shards, s, x, *traffic) for s in range(2)]
+    half = shards // 2
 
     def prepare(m):
         loads[m].wait()
-
-        @pl.loop(0, raw.shape[2] // LANES)
-        def _(c):
-            span = lanes_of(c, LANES)
+        for c in range(raw.shape[2] // LANES):
+            span = pl.ds(c * LANES, LANES)
             block = raw[m, :, span].T
             if m % 3 < 2:
                 block = block * gains[m // 3][...]
             turned[m, span, :] = block.astype(jnp.bfloat16)
 
-        moves.send(m)
-
-    moves = HandOver(shards, sources, held, land, first, onward)
-    steps = [Tokens(shards, s, x, *traffic) for s in range(2)]
-    store = [pltpu.make_async_copy(held.at[m], outs[m], written.at[m]) for m in range(6)]
+    def send(m):
+        for k in range(half):
+            moves.send(m, k)
+
+    def near(m):
+        for i in range(half):
+            moves.relay_near(m, i)
+
+    def far(m):
+        for i in range(half):
+            moves.relay_far(m, i)
+
     for load in loads:
         load.start()
-    greet(shards)
+    ready = greet(shards)
+    prepare(0)
+    ready()
     start = pltpu.make_async_copy(prompt, steps[0].piece(steps[0].f), alone.at[0])
     start.start()
     steps[0].spread(prompt)
-    for m in range(3):
-        prepare(m)
-    moves.relay_near(0)
-    steps[0].pass_on()
-    moves.relay_near(1)
-    moves.relay_far(0)
+    send(0)
+    prepare(1)
+    prepare(2)
     prepare(3)
-    moves.relay_near(2)
-    moves.relay_far(1)
-    moves.relay_far(2)
-    for m in range(3):
-        moves.settle(m)
-        store[m].start()
+    prepare(4)
+    prepare(5)
+    steps[0].pass_on(0)
+    send(1)
+    near(0)
+    send(2)
+    steps[0].pass_on(1)
+    for i in range(half):
+        moves.relay_far(0, i)
+        moves.relay_near(1, i)
+    send(3)
+    steps[0].pass_on(2)
+    for i in range(half):
+        moves.relay_near(2, i)
+        moves.relay_far(1, i)
     start.wait()
     steps[0].collect()
-    steps[0].activate(held.at[0], held.at[1], hidden, features)
-    steps[0].reduce_pairs(hidden, held.at[2])
-    prepare(4)
-    moves.relay_near(3)
-    steps[0].reduce_outer(hidden, held.at[2], own)
-    prepare(5)
-    moves.relay_far(3)
+    for m in range(2):
+        moves.settle(m)
+    steps[0].activate(held[0], held[1], hidden, features)
+    far(2)
+    moves.settle(2)
+    for k in range(4):
+        steps[0].swap(hidden, held[2], k)
+    for k in range(4):
+        steps[0].gather_term(hidden, held[2], own, k)
+    moves.send(4, 0)
+    near(3)
+    steps[0].reduce(own, 0)
+    moves.send(4, 1)
+    steps[0].reduce(own, 1)
+    moves.send(4, 2)
+    moves.send(4, 3)
+    steps[0].reduce(own, 2)
+    moves.send(5, 0)
+    moves.send(5, 1)
     tokens = steps[0].finish(own, units)
     middle[...] = tokens
     x[1, :, lanes_of(steps[1].f, steps[1].width)] = tokens
     steps[1].spread(middle)
-    moves.relay_near(4)
-    steps[1].pass_on()
-    moves.relay_near(5)
-    moves.relay_far(4)
-    moves.relay_far(5)
-    for m in range(3, 6):
+    moves.send(5, 2)
+    far(3)
+    steps[1].pass_on(0)
+    moves.send(5, 3)
+    near(4)
+    steps[1].pass_on(1)
+    far(4)
+    steps[1].pass_on(2)
+    near(5)
+    steps[1].collect()
+    for m in range(3, 5):
         moves.settle(m)
-        store[m].start()
-    steps[1].collect()
-    steps[1].activate(held.at[3], held.at[4], hidden, features)
-    steps[1].reduce_pairs(hidden, held.at[5])
-    steps[1].reduce_outer(hidden, held.at[5], own)
-    last[...] = steps[1].finish(own, units)
-    end = pltpu.make_async_copy(last, result, alone.at[1])
-    end.start()
+    steps[1].activate(held[3], held[4], hidden, features)
+    far(5)
+    moves.settle(5)
+    for k in range(4):
+        steps[1].swap(hidden, held[5], k)
+    for k in range(4):
+        steps[1].gather_term(hidden, held[5], own, k)
+    steps[1].reduce(own, 0)
+    steps[1].reduce(own, 1)
+    steps[1].reduce(own, 2)
+    result[...] = steps[1].finish(own, units)
     for m in range(6):
         moves.drain(m)
-        store[m].wait()
     for step in steps:
         step.drain()
-    end.wait()
 
 
 def whole(prompt, gains, trained, shards):
@@ -340,21 +380,19 @@
     rows, width = prompt.shape
     depth = shards // 2
     any_space = pl.BlockSpec(memory_space=pl.ANY)
+    vmem = pl.BlockSpec(memory_space=pltpu.VMEM)
     return pl.pallas_call(
         functools.partial(whole_kernel, shards, features, units),
-        out_shape=[jax.ShapeDtypeStruct(prompt.shape, jnp.bfloat16)] + [jax.ShapeDtypeStruct((height, features), jnp.bfloat16)] * 6,
-        in_specs=[any_space] + [pl.BlockSpec(memory_space=pltpu.VMEM)] * 2 + [any_space] * 6,
-        out_specs=[any_space] * 7,
+        out_shape=[pltpu.VMEM(prompt.shape, jnp.bfloat16)] + [pltpu.VMEM((height, features), jnp.bfloat16)] * 6,
+        in_specs=[any_space] + [vmem] * 2 + [any_space] * 6,
+        out_specs=[vmem] * 7,
         scratch_shapes=[
-            pltpu.VMEM((6, height, features), jnp.bfloat16),
             pltpu.SemaphoreType.DMA((6, 2 * shards)),
             pltpu.SemaphoreType.DMA((6, shards // 2)),
             pltpu.SemaphoreType.DMA((6, 3 * shards // 2)),
-            pltpu.SemaphoreType.DMA((6,)),
             pltpu.VMEM((2, rows, features), jnp.bfloat16),
             pltpu.VMEM((rows, height), jnp.bfloat16),
             pltpu.VMEM((depth, rows, width), jnp.float32),
-            pltpu.VMEM((rows, width), jnp.bfloat16),
             pltpu.VMEM((rows, width), jnp.bfloat16),
             pltpu.SemaphoreType.DMA((2, shards)),
             pltpu.SemaphoreType.DMA((2, 4 * depth)),
@@ -366,12 +404,12 @@
             pltpu.VMEM((2, 2, depth, rows, width), jnp.bfloat16),
             pltpu.SemaphoreType.DMA((2, depth)),
             pltpu.SemaphoreType.DMA((2, 2, depth)),
-            pltpu.SemaphoreType.DMA((2,)),
+            pltpu.SemaphoreType.DMA((1,)),
             pltpu.VMEM((6,) + trained[0].shape, jnp.float32),
             pltpu.VMEM((6, trained[0].shape[1], LANES), jnp.bfloat16),
             pltpu.SemaphoreType.DMA((6,)),
         ],
-        compiler_params=pltpu.CompilerParams(collective_id=0, has_side_effects=True, vmem_limit_bytes=60 << 20),
+        compiler_params=pltpu.CompilerParams(collective_id=0, has_side_effects=True, vmem_limit_bytes=40 << 20),
     )(prompt, *gains, *trained)
 
 

time: 264 us -> 217 us (0.82)
  Pallas kernels: 244 us -> 206 us
  local copies, waits for them, and re-layouts: 18.6 us -> 10.2 us
    pallas_call x1, Pallas kernels: 244 us -> 206 us  [whole(): pl.pallas_call(functools.partial(whole_kernel, shards, features, units),...]
    unnamed x17 -> x7, local copies, waits for them, and re-layouts: 18.6 us -> 10.2 us
where the time goes in v1:
time: 217 us
  Pallas kernels  206 us (95%)
  local copies, waits for them, and re-layouts  10.2 us (5%)
    pallas_call x1, Pallas kernels, whole(): pl.pallas_call(functools.partial(whole_kernel, shards, features, units),...  206 us
    unnamed x7, local copies, waits for them, and re-layouts  10.2 us

profile of v1, /device:TPU:0, one launch (start us, length us, event | category | flops | bytes accessed | tf_op | source)
XLA Modules:
  0.0 216.7 jit_solution(12278629218012948115)
XLA Ops:
  0.6 205.9 %shard_map.144 = (bf16[512,256]{1,0:T(8,128)(2,1)S(1)}, bf16[704,2048]{1,0:T(8,128)(2,1)S(1)}, bf16[704,2048]{1,0:T(8,128)(2,1)S(1)}, bf16[704,2048]{1,0:T(8,128...) custom-call(bf16[512,256]{1,0:T(8,128)(2,1)} %refs_0_.1, ...), custom_call_target="tpu_custom_call" | custom-call | tf_op jit(solution)/shard_map/pallas_call | solution.py:384
  206.5 0.7 copy.23
  207.2 1.6 copy.24
  208.8 1.6 copy.25
  210.4 1.6 copy.26
  211.9 1.6 copy.27
  213.5 1.6 copy.28
  215.1 1.6 copy.29

commit v2 on v1

--- a/solution.py
+++ b/solution.py
@@ -13,6 +13,16 @@
 
 def lanes_of(block, width):
     return pl.ds(pl.multiple_of(block * width, width), width)
+
+
+def place_of(count, here, k):
+    low = here < count // 2
+    z = jnp.where(low, here, count - 1 - here)
+    j = k - (count - 1 - 2 * z)
+    late = jnp.maximum(j, 0)
+    nearby = z + (1 - 2 * lax.rem(late, 2)) * (z - late // 2)
+    found = jnp.where(j < 0, count - 1 - k, nearby)
+    return jnp.where(low, found, count - 1 - found)
 
 
 class HandOver:
@@ -40,7 +50,7 @@
         home = lax.rem(self.f, 2)
         target = self.t * self.half + k
         column = self.g * self.n + self.f
-        block = self.sources[m].at[pl.ds(k * self.height, self.height), :]
+        block = self.sources[m].at[pl.ds(pl.multiple_of(k * self.height, 16), self.height), :]
         stays = jnp.logical_and(target == self.f, home == self.t)
 
         @pl.when(jnp.logical_not(stays))
@@ -70,12 +80,14 @@
     def far(self, i):
         return (1 - self.g) * self.n + 2 * i + self.t
 
-    def relay_near(self, m, i):
+    def relay_near(self, m, j):
+        i = place_of(self.half, self.f // 2, self.half - 1 - j)
         self.arrived(m, self.near(i))
         self.forward(m, i, self.near(i), 0).start()
         self.forward(m, i, self.near(i), 1).start()
 
-    def relay_far(self, m, i):
+    def relay_far(self, m, j):
+        i = place_of(self.half, self.f // 2, self.half - 1 - j)
         self.arrived(m, self.far(i))
         self.forward(m, i, self.far(i), 2).start()
 
@@ -103,16 +115,23 @@
     return lambda: pl.semaphore_wait(barrier, 2 * shards)
 
 
+CHUNKS = 4
+
+
 class Tokens:
     def __init__(self, shards, step, x, gathered, gather_out, over_y, into_y, y_out, y_in, over_z, into_z, z_out, z_in):
-        self.n, self.depth, self.step = shards, shards // 2, step
-        self.x, self.gathered, self.gather_out = x.at[step], gathered, gather_out
-        self.over_y, self.into_y, self.y_out, self.y_in = over_y, into_y, y_out, y_in
-        self.over_z, self.into_z, self.z_out, self.z_in = over_z, into_z, z_out, z_in
+        self.n, self.depth = shards, shards // 2
+        self.x, self.gathered, self.gather_out = x.at[step], gathered.at[step], gather_out.at[step]
+        self.over_y, self.into_y, self.y_out, self.y_in = over_y.at[step], into_y.at[step], y_out.at[step], y_in.at[step]
+        self.over_z, self.into_z, self.z_out, self.z_in = over_z.at[step], into_z.at[step], z_out.at[step], z_in.at[step]
         self.g, self.f, self.t = lax.axis_index("gr"), lax.axis_index("fs"), lax.axis_index("tp")
         self.z, self.y = self.f // 2, lax.rem(self.f, 2)
         self.width = over_y.shape[-1]
+        self.rows = x.shape[1] // CHUNKS
         self.sent = []
+
+    def span(self, c):
+        return pl.ds(c * self.rows, self.rows)
 
     def go(self, when, make):
         @pl.when(when)
@@ -131,22 +150,23 @@
             device_id_type=MESH,
         )
 
-    def piece(self, owner):
-        return self.x.at[:, lanes_of(owner, self.width)]
-
-    def hand_on(self, when, source, owner, sem, target):
-        self.go(when, lambda: self.copy(source(), self.piece(owner), self.gather_out.at[self.step, sem], self.gathered.at[self.step, owner], target))
-
-    def spread(self, own):
-        self.hand_on(self.z < self.depth - 1, lambda: own, self.f, 0, self.f + 2)
-        self.hand_on(self.z > 0, lambda: own, self.f, 1, self.f - 2)
-        self.hand_on(self.z >= 0, lambda: own, self.f, 2, 2 * self.z + 1 - self.y)
-
-    def came(self, owner):
-        piece = self.piece(owner)
-        pltpu.make_async_copy(piece, piece, self.gathered.at[self.step, owner]).wait()
-
-    def pass_on(self, i):
+    def piece(self, owner, c):
+        return self.x.at[self.span(c), lanes_of(owner, self.width)]
+
+    def hand_on(self, when, source, owner, sem, target, c):
+        self.go(when, lambda: self.copy(source(), self.piece(owner, c), self.gather_out.at[c, sem], self.gathered.at[c, owner], target))
+
+    def spread(self, own, c):
+        source = own.at[self.span(c), :]
+        self.hand_on(self.z < self.depth - 1, lambda: source, self.f, 0, self.f + 2, c)
+        self.hand_on(self.z > 0, lambda: source, self.f, 1, self.f - 2, c)
+        self.hand_on(self.z >= 0, lambda: source, self.f, 2, 2 * self.z + 1 - self.y, c)
+
+    def came(self, owner, c):
+        piece = self.piece(owner, c)
+        pltpu.make_async_copy(piece, piece, self.gathered.at[c, owner]).wait()
+
+    def pass_on(self, i, c):
         for side, sign in enumerate((-1, 1)):
             place = self.z + sign * (1 + i)
             owner = 2 * place + self.y
@@ -156,14 +176,15 @@
 
             @pl.when(there)
             def _(owner=owner):
-                self.came(owner)
-
-            self.hand_on(further, lambda owner=owner: self.piece(owner), owner, sem, self.f - 2 * sign)
-            self.hand_on(there, lambda owner=owner: self.piece(owner), owner, sem + 1, 2 * self.z + 1 - self.y)
+                self.came(owner, c)
+
+            self.hand_on(further, lambda owner=owner: self.piece(owner, c), owner, sem, self.f - 2 * sign, c)
+            self.hand_on(there, lambda owner=owner: self.piece(owner, c), owner, sem + 1, 2 * self.z + 1 - self.y, c)
 
     def collect(self):
         for i in range(self.depth):
-            self.came(2 * i + 1 - self.y)
+            for c in range(CHUNKS):
+                self.came(2 * i + 1 - self.y, c)
 
     def activate(self, w_gate, w_up, hidden, features):
         rows = self.x.shape[0]
@@ -185,52 +206,46 @@
         return jnp.dot(hidden[...], w_down[:, lanes_of(owner, self.width)], preferred_element_type=jnp.float32)
 
     def place(self, k):
-        n = self.depth
-        low = self.z < n // 2
-        z = jnp.where(low, self.z, n - 1 - self.z)
-        lead = n - 1 - 2 * z
-        j = k - lead
-        nearby = z + (1 - 2 * lax.rem(jnp.maximum(j, 0), 2)) * (z - jnp.maximum(j, 0) // 2)
-        found = jnp.where(j < 0, n - 1 - k, nearby)
-        return jnp.where(low, found, n - 1 - found)
+        return place_of(self.depth, self.z, k)
 
     def swap(self, hidden, w_down, k):
-        s = self.step
-        self.over_y[s, k] = self.term(hidden, w_down, 2 * self.place(k) + 1 - self.y).astype(jnp.bfloat16)
-        self.go(
-            self.z >= 0,
-            lambda: self.copy(self.over_y.at[s, k], self.into_y.at[s, k], self.y_out.at[s, k], self.y_in.at[s, k], 2 * self.z + 1 - self.y),
-        )
+        self.over_y[k] = self.term(hidden, w_down, 2 * self.place(k) + 1 - self.y).astype(jnp.bfloat16)
+        for c in range(CHUNKS):
+            part = (k, self.span(c))
+            self.go(
+                self.z >= 0,
+                lambda c=c, part=part: self.copy(self.over_y.at[part], self.into_y.at[part], self.y_out.at[c, k], self.y_in.at[c, k], 2 * self.z + 1 - self.y),
+            )
 
     def gather_term(self, hidden, w_down, own, k):
-        s = self.step
         own[k] = self.term(hidden, w_down, 2 * self.place(k) + self.y)
 
-    def reduce(self, own, k):
-        s = self.step
+    def reduce(self, own, k, c):
         place = self.place(k)
         up = place > self.z
         side = jnp.where(up, 0, 1)
         inner = jnp.where(up, self.z, self.depth - 1 - self.z) > 0
-        self.wait(self.into_y.at[s, k], self.y_in.at[s, k])
+        part = (k, self.span(c))
+        passed = (side, place, self.span(c))
+        self.wait(self.into_y.at[part], self.y_in.at[c, k])
 
         @pl.when(inner)
         def _():
-            self.wait(self.into_z.at[s, side, place], self.z_in.at[s, side, place])
-            total = own[k] + self.into_y[s, k].astype(jnp.float32) + self.into_z[s, side, place].astype(jnp.float32)
-            self.over_z[s, k] = total.astype(jnp.bfloat16)
+            self.wait(self.into_z.at[passed], self.z_in.at[c, side, place])
+            total = own[part] + self.into_y[part].astype(jnp.float32) + self.into_z[passed].astype(jnp.float32)
+            self.over_z[part] = total.astype(jnp.bfloat16)
 
         @pl.when(jnp.logical_not(inner))
         def _():
-            self.over_z[s, k] = (own[k] + self.into_y[s, k].astype(jnp.float32)).astype(jnp.bfloat16)
+            self.over_z[part] = (own[part] + self.into_y[part].astype(jnp.float32)).astype(jnp.bfloat16)
 
         self.go(
             self.z >= 0,
             lambda: self.copy(
-                self.over_z.at[s, k],
-                self.into_z.at[s, side, place],
-                self.z_out.at[s, k],
-                self.z_in.at[s, side, place],
+                self.over_z.at[part],
+                self.into_z.at[passed],
+                self.z_out.at[c, k],
+                self.z_in.at[c, side, place],
                 self.f + 2 - 4 * side,
             ),
         )
@@ -238,20 +253,22 @@
     def wait(self, landed, sem):
         pltpu.make_async_copy(landed, landed, sem).wait()
 
-    def finish(self, own, units):
-        s, k = self.step, self.depth - 1
-        self.wait(self.into_y.at[s, k], self.y_in.at[s, k])
-        own[k] += self.into_y[s, k].astype(jnp.float32)
+    def finish(self, own, units, c):
+        k = self.depth - 1
+        part = (k, self.span(c))
+        self.wait(self.into_y.at[part], self.y_in.at[c, k])
+        own[part] += self.into_y[part].astype(jnp.float32)
         for side in range(2):
             inner = self.z > 0 if side == 0 else self.z < self.depth - 1
 
             @pl.when(inner)
             def _(side=side):
-                self.wait(self.into_z.at[s, side, self.z], self.z_in.at[s, side, self.z])
-                own[k] += self.into_z[s, side, self.z].astype(jnp.float32)
-
-        before = self.x[:, lanes_of(self.f, self.width)].astype(jnp.float32)
-        return (before + 0.5 * units ** (-0.5) * own[k]).astype(jnp.bfloat16)
+                passed = (side, self.z, self.span(c))
+                self.wait(self.into_z.at[passed], self.z_in.at[c, side, self.z])
+                own[part] += self.into_z[passed].astype(jnp.float32)
+
+        before = self.x[self.span(c), lanes_of(self.f, self.width)].astype(jnp.float32)
+        return (before + 0.5 * units ** (-0.5) * own[part]).astype(jnp.bfloat16)
 
     def drain(self):
         for when, make in self.sent:
@@ -268,8 +285,8 @@
     sources = [turned.at[m] for m in range(6)]
     loads = [pltpu.make_async_copy(trained[m], raw.at[m], loaded.at[m]) for m in range(6)]
     moves = HandOver(shards, sources, held, land, first, onward)
-    steps = [Tokens(shards, s, x, *traffic) for s in range(2)]
     half = shards // 2
+    tokens = [Tokens(shards, step, x, *traffic) for step in range(2)]
 
     def prepare(m):
         loads[m].wait()
@@ -284,93 +301,203 @@
         for k in range(half):
             moves.send(m, k)
 
-    def near(m):
-        for i in range(half):
-            moves.relay_near(m, i)
-
-    def far(m):
-        for i in range(half):
-            moves.relay_far(m, i)
+    row = lax.rem(moves.f, 2)
+    turning = row != moves.t
+
+    def send_turning(m):
+        for j in range(half // 2):
+            moves.send(m, 2 * j + 1 - row)
+
+    def send_straight(m):
+        for j in range(half // 2):
+            moves.send(m, 2 * j + row)
+
+    def near_if(m, turned_row):
+        @pl.when(turning if turned_row else jnp.logical_not(turning))
+        def _():
+            for i in range(half):
+                moves.relay_near(m, i)
+
+    def far_if(m, turned_row):
+        @pl.when(turning if turned_row else jnp.logical_not(turning))
+        def _():
+            for i in range(half):
+                moves.relay_far(m, i)
+
+    def spread(step, own_tokens):
+        for c in range(CHUNKS):
+            tokens[step].spread(own_tokens, c)
+
+    def pass_on(step, i):
+        for c in range(CHUNKS):
+            tokens[step].pass_on(i, c)
+
+    def activate(step):
+        tokens[step].activate(held[3 * step], held[3 * step + 1], hidden, features)
+
+    def swap(step):
+        for k in range(half):
+            tokens[step].swap(hidden, held[3 * step + 2], k)
+
+    def terms(step):
+        for k in range(half):
+            tokens[step].gather_term(hidden, held[3 * step + 2], own, k)
+
+    def reduce(step, k):
+        for c in range(CHUNKS):
+            tokens[step].reduce(own, k, c)
+
+    def hand_back():
+        for c in range(CHUNKS):
+            span = tokens[0].span(c)
+            done = tokens[0].finish(own, units, c)
+            middle[span, :] = done
+            x[1, span, lanes_of(tokens[1].f, tokens[1].width)] = done
+            tokens[1].spread(middle, c)
+
+    def deliver():
+        for c in range(CHUNKS):
+            result[tokens[1].span(c), :] = tokens[1].finish(own, units, c)
 
     for load in loads:
         load.start()
     ready = greet(shards)
     prepare(0)
     ready()
-    start = pltpu.make_async_copy(prompt, steps[0].piece(steps[0].f), alone.at[0])
+    start = pltpu.make_async_copy(prompt, x.at[0, :, lanes_of(moves.f, prompt.shape[1])], alone.at[0])
     start.start()
-    steps[0].spread(prompt)
-    send(0)
+    spread(0, prompt)
+    moves.send(0, 0)
+    moves.send(0, 1)
+    moves.send(0, 2)
+    moves.send(0, 3)
     prepare(1)
     prepare(2)
     prepare(3)
     prepare(4)
     prepare(5)
-    steps[0].pass_on(0)
-    send(1)
-    near(0)
-    send(2)
-    steps[0].pass_on(1)
-    for i in range(half):
-        moves.relay_far(0, i)
-        moves.relay_near(1, i)
-    send(3)
-    steps[0].pass_on(2)
-    for i in range(half):
-        moves.relay_near(2, i)
-        moves.relay_far(1, i)
+    pass_on(0, 0)
+    moves.send(1, 0)
+    moves.send(1, 1)
+    moves.relay_near(0, 0)
+    moves.relay_near(0, 1)
+    moves.relay_near(0, 2)
+    pass_on(0, 1)
+    moves.relay_near(0, 3)
+    moves.send(1, 2)
+    moves.send(1, 3)
+    moves.relay_near(1, 0)
+    moves.relay_near(1, 1)
+    moves.relay_near(1, 2)
+    moves.send(2, 0)
+    moves.send(2, 1)
+    pass_on(0, 2)
+    moves.relay_near(1, 3)
+    moves.send(2, 2)
+    moves.send(2, 3)
+    moves.relay_far(0, 0)
+    moves.relay_far(0, 1)
+    moves.relay_far(0, 2)
+    moves.relay_far(0, 3)
+    moves.relay_near(2, 0)
+    moves.relay_near(2, 1)
+    moves.relay_near(2, 2)
+    moves.send(3, 0)
+    moves.send(3, 1)
+    moves.send(3, 2)
+    moves.send(3, 3)
+    moves.relay_near(2, 3)
+    moves.relay_far(1, 0)
+    moves.relay_far(1, 1)
+    moves.relay_far(1, 2)
+    moves.relay_far(1, 3)
     start.wait()
-    steps[0].collect()
-    for m in range(2):
-        moves.settle(m)
-    steps[0].activate(held[0], held[1], hidden, features)
-    far(2)
-    moves.settle(2)
-    for k in range(4):
-        steps[0].swap(hidden, held[2], k)
-    for k in range(4):
-        steps[0].gather_term(hidden, held[2], own, k)
+    tokens[0].collect()
+    moves.settle(0)
+    moves.settle(1)
+    activate(0)
     moves.send(4, 0)
-    near(3)
-    steps[0].reduce(own, 0)
     moves.send(4, 1)
-    steps[0].reduce(own, 1)
     moves.send(4, 2)
     moves.send(4, 3)
-    steps[0].reduce(own, 2)
+    moves.relay_far(2, 0)
+    moves.relay_far(2, 1)
+    moves.relay_far(2, 2)
+    moves.relay_far(2, 3)
+    moves.settle(2)
+    swap(0)
+    terms(0)
     moves.send(5, 0)
     moves.send(5, 1)
-    tokens = steps[0].finish(own, units)
-    middle[...] = tokens
-    x[1, :, lanes_of(steps[1].f, steps[1].width)] = tokens
-    steps[1].spread(middle)
     moves.send(5, 2)
-    far(3)
-    steps[1].pass_on(0)
     moves.send(5, 3)
-    near(4)
-    steps[1].pass_on(1)
-    far(4)
-    steps[1].pass_on(2)
-    near(5)
-    steps[1].collect()
-    for m in range(3, 5):
-        moves.settle(m)
-    steps[1].activate(held[3], held[4], hidden, features)
-    far(5)
+    moves.relay_near(3, 0)
+    moves.relay_near(3, 1)
+    moves.relay_near(3, 2)
+    moves.relay_near(3, 3)
+    reduce(0, 0)
+    reduce(0, 1)
+    moves.relay_near(4, 0)
+    moves.relay_near(4, 1)
+    moves.relay_near(4, 2)
+    moves.relay_near(4, 3)
+    reduce(0, 2)
+    hand_back()
+    moves.relay_far(3, 0)
+    moves.relay_far(3, 1)
+    moves.relay_far(3, 2)
+    moves.relay_far(3, 3)
+    moves.relay_near(5, 0)
+    moves.relay_near(5, 1)
+    moves.relay_near(5, 2)
+    moves.relay_near(5, 3)
+    pass_on(1, 0)
+    moves.relay_far(4, 0)
+    moves.relay_far(4, 1)
+    moves.relay_far(4, 2)
+    moves.relay_far(4, 3)
+    pass_on(1, 1)
+    moves.relay_far(5, 0)
+    moves.relay_far(5, 1)
+    moves.relay_far(5, 2)
+    moves.relay_far(5, 3)
+    pass_on(1, 2)
+    tokens[1].collect()
+    moves.settle(3)
+    moves.settle(4)
+    activate(1)
     moves.settle(5)
-    for k in range(4):
-        steps[1].swap(hidden, held[5], k)
-    for k in range(4):
-        steps[1].gather_term(hidden, held[5], own, k)
-    steps[1].reduce(own, 0)
-    steps[1].reduce(own, 1)
-    steps[1].reduce(own, 2)
-    result[...] = steps[1].finish(own, units)
+    swap(1)
+    terms(1)
+    reduce(1, 0)
+    reduce(1, 1)
+    reduce(1, 2)
+    deliver()
     for m in range(6):
         moves.drain(m)
-    for step in steps:
-        step.drain()
+    for part in tokens:
+        part.drain()
+
+
+def write_kernel(count, *refs):
+    sources, outs, written = refs[:count], refs[count : 2 * count], refs[2 * count]
+    copies = [pltpu.make_async_copy(sources[i], outs[i], written.at[i]) for i in range(count)]
+    for copy in copies:
+        copy.start()
+    for copy in copies:
+        copy.wait()
+
+
+def write_out(arrays):
+    count = len(arrays)
+    return pl.pallas_call(
+        functools.partial(write_kernel, count),
+        out_shape=[jax.ShapeDtypeStruct(a.shape, a.dtype) for a in arrays],
+        in_specs=[pl.BlockSpec(memory_space=pltpu.VMEM)] * count,
+        out_specs=[pl.BlockSpec(memory_space=pl.ANY)] * count,
+        scratch_shapes=[pltpu.SemaphoreType.DMA((count,))],
+        compiler_params=pltpu.CompilerParams(vmem_limit_bytes=1 << 20),
+    )(*[pltpu.with_memory_space_constraint(a, pltpu.VMEM) for a in arrays])
 
 
 def whole(prompt, gains, trained, shards):
@@ -381,7 +508,7 @@
     depth = shards // 2
     any_space = pl.BlockSpec(memory_space=pl.ANY)
     vmem = pl.BlockSpec(memory_space=pltpu.VMEM)
-    return pl.pallas_call(
+    outs = pl.pallas_call(
         functools.partial(whole_kernel, shards, features, units),
         out_shape=[pltpu.VMEM(prompt.shape, jnp.bfloat16)] + [pltpu.VMEM((height, features), jnp.bfloat16)] * 6,
         in_specs=[any_space] + [vmem] * 2 + [any_space] * 6,
@@ -394,23 +521,24 @@
             pltpu.VMEM((rows, height), jnp.bfloat16),
             pltpu.VMEM((depth, rows, width), jnp.float32),
             pltpu.VMEM((rows, width), jnp.bfloat16),
-            pltpu.SemaphoreType.DMA((2, shards)),
-            pltpu.SemaphoreType.DMA((2, 4 * depth)),
+            pltpu.SemaphoreType.DMA((2, CHUNKS, shards)),
+            pltpu.SemaphoreType.DMA((2, CHUNKS, 4 * depth)),
             pltpu.VMEM((2, depth, rows, width), jnp.bfloat16),
             pltpu.VMEM((2, depth, rows, width), jnp.bfloat16),
-            pltpu.SemaphoreType.DMA((2, depth)),
-            pltpu.SemaphoreType.DMA((2, depth)),
+            pltpu.SemaphoreType.DMA((2, CHUNKS, depth)),
+            pltpu.SemaphoreType.DMA((2, CHUNKS, depth)),
             pltpu.VMEM((2, depth, rows, width), jnp.bfloat16),
             pltpu.VMEM((2, 2, depth, rows, width), jnp.bfloat16),
-            pltpu.SemaphoreType.DMA((2, depth)),
-            pltpu.SemaphoreType.DMA((2, 2, depth)),
+            pltpu.SemaphoreType.DMA((2, CHUNKS, depth)),
+            pltpu.SemaphoreType.DMA((2, CHUNKS, 2, depth)),
             pltpu.SemaphoreType.DMA((1,)),
             pltpu.VMEM((6,) + trained[0].shape, jnp.float32),
             pltpu.VMEM((6, trained[0].shape[1], LANES), jnp.bfloat16),
             pltpu.SemaphoreType.DMA((6,)),
         ],
-        compiler_params=pltpu.CompilerParams(collective_id=0, has_side_effects=True, vmem_limit_bytes=40 << 20),
+        compiler_params=pltpu.CompilerParams(collective_id=0, has_side_effects=True, vmem_limit_bytes=42 << 20),
     )(prompt, *gains, *trained)
+    return write_out(outs)
 
 
 D = 2048
@@ -513,7 +641,7 @@
     shards = lax.axis_size("fs")
     units = shape[1] * lax.axis_size("tp")
     whole_rows = shape[0] == LANES and shape[1] % LANES == 0 and units % (16 * shards) == 0
-    whole_tokens = token_shape[0] % 32 == 0 and token_shape[1] % LANES == 0
+    whole_tokens = token_shape[0] % (32 * CHUNKS) == 0 and token_shape[1] % LANES == 0
     pairs = shards % 4 == 0 and lax.axis_size("gr") == 2 and lax.axis_size("tp") == 2
     return whole_rows and whole_tokens and pairs
 

time: 217 us -> 188 us (0.87)
  Pallas kernels: 206 us -> 188 us
  local copies, waits for them, and re-layouts: 10.2 us -> 0 us
    pallas_call x1, Pallas kernels: 206 us -> 181 us  [whole(): pl.pallas_call(functools.partial(whole_kernel, shards, features, units),...]
    unnamed x7 -> x0, local copies, waits for them, and re-layouts: 10.2 us -> none
    pallas_call x0 -> x1, Pallas kernels: none -> 6.23 us  [write_out(): pl.pallas_call(functools.partial(write_kernel, count), out_shape=[jax.Sha...]
where the time goes in v2:
time: 188 us
  Pallas kernels  188 us (100%)
    pallas_call x1, Pallas kernels, whole(): pl.pallas_call(functools.partial(whole_kernel, shards, features, units),...  181 us
    pallas_call x1, Pallas kernels, write_out(): pl.pallas_call(functools.partial(write_kernel, count), out_shape=[jax.Sha...  6.23 us

profile of v2, /device:TPU:0, one launch (start us, length us, event | category | flops | bytes accessed | tf_op | source)
XLA Modules:
  0.0 188.3 jit_solution(15688611474352203048)
XLA Ops:
  0.6 181.3 %shard_map.144 = (bf16[512,256]{1,0:T(8,128)(2,1)S(1)}, bf16[704,2048]{1,0:T(8,128)(2,1)S(1)}, bf16[704,2048]{1,0:T(8,128)(2,1)S(1)}, bf16[704,2048]{1,0:T(8,128...) custom-call(bf16[512,256]{1,0:T(8,128)(2,1)} %refs_0_.1, ...), custom_call_target="tpu_custom_call" | custom-call | tf_op jit(solution)/shard_map/pallas_call | solution.py:511
  181.9 6.2 %shard_map.145 = (bf16[512,256]{1,0:T(8,128)(2,1)}, bf16[704,2048]{1,0:T(8,128)(2,1)}, bf16[704,2048]{1,0:T(8,128)(2,1)}, bf16[704,2048]{1,0:T(8,128)(2,1)}, bf1...) custom-call(bf16[512,256]{1,0:T(8,128)(2,1)S(1)} %get-tuple-element.14.refs_0_, ...), custom_call_target="tpu_custom_call" | custom-call | tf_op jit(solution)/shard_map/pallas_call | solution.py:493

commit v3 on v2

--- a/solution.py
+++ b/solution.py
@@ -116,6 +116,15 @@
 
 
 CHUNKS = 4
+PLACES = 4
+
+
+def chunks_of(h):
+    return range(h * CHUNKS // 2, (h + 1) * CHUNKS // 2)
+
+
+def half_of(h, rows):
+    return pl.ds(h * rows // 2, rows // 2)
 
 
 class Tokens:
@@ -181,26 +190,21 @@
             self.hand_on(further, lambda owner=owner: self.piece(owner, c), owner, sem, self.f - 2 * sign, c)
             self.hand_on(there, lambda owner=owner: self.piece(owner, c), owner, sem + 1, 2 * self.z + 1 - self.y, c)
 
-    def collect(self):
+    def collect(self, h):
         for i in range(self.depth):
-            for c in range(CHUNKS):
+            for c in chunks_of(h):
                 self.came(2 * i + 1 - self.y, c)
 
-    def activate(self, w_gate, w_up, hidden, features):
-        rows = self.x.shape[0]
-        chunk = rows // 2
-
-        @pl.loop(0, 2)
-        def _(c):
-            span = pl.ds(pl.multiple_of(c * chunk, chunk), chunk)
-            tokens = self.x[span, :]
-            widened = tokens.astype(jnp.float32)
-            squares = jnp.sum(widened * widened, axis=1, keepdims=True)
-            scale = lax.rsqrt(squares / features + norm_eps) * features ** (-0.5)
-            dims = (((1,), (1,)), ((), ()))
-            gate = lax.dot_general(tokens, w_gate[...], dims, preferred_element_type=jnp.float32) * scale
-            up = lax.dot_general(tokens, w_up[...], dims, preferred_element_type=jnp.float32) * scale
-            hidden[span, :] = (gate / (1.0 + jnp.exp(-gate)) * up).astype(jnp.bfloat16)
+    def activate(self, w_gate, w_up, hidden, features, h):
+        span = half_of(h, self.x.shape[0])
+        tokens = self.x[span, :]
+        widened = tokens.astype(jnp.float32)
+        squares = jnp.sum(widened * widened, axis=1, keepdims=True)
+        scale = lax.rsqrt(squares / features + norm_eps) * features ** (-0.5)
+        dims = (((1,), (1,)), ((), ()))
+        gate = lax.dot_general(tokens, w_gate[...], dims, preferred_element_type=jnp.float32) * scale
+        up = lax.dot_general(tokens, w_up[...], dims, preferred_element_type=jnp.float32) * scale
+        hidden[span, :] = (gate / (1.0 + jnp.exp(-gate)) * up).astype(jnp.bfloat16)
 
     def term(self, hidden, w_down, owner):
         return jnp.dot(hidden[...], w_down[:, lanes_of(owner, self.width)], preferred_element_type=jnp.float32)
@@ -208,9 +212,10 @@
     def place(self, k):
         return place_of(self.depth, self.z, k)
 
-    def swap(self, hidden, w_down, k):
-        self.over_y[k] = self.term(hidden, w_down, 2 * self.place(k) + 1 - self.y).astype(jnp.bfloat16)
-        for c in range(CHUNKS):
+    def swap(self, hidden, w_down, k, h):
+        span = half_of(h, self.x.shape[0])
+        self.over_y[k, span] = self.term(hidden.at[span, :], w_down, 2 * self.place(k) + 1 - self.y).astype(jnp.bfloat16)
+        for c in chunks_of(h):
             part = (k, self.span(c))
             self.go(
                 self.z >= 0,
@@ -332,19 +337,21 @@
         for c in range(CHUNKS):
             tokens[step].pass_on(i, c)
 
-    def activate(step):
-        tokens[step].activate(held[3 * step], held[3 * step + 1], hidden, features)
-
-    def swap(step):
-        for k in range(half):
-            tokens[step].swap(hidden, held[3 * step + 2], k)
+    def collect(step, h):
+        tokens[step].collect(h)
+
+    def activate(step, h):
+        tokens[step].activate(held[3 * step], held[3 * step + 1], hidden, features, h)
+
+    def swap(step, k, h):
+        tokens[step].swap(hidden, held[3 * step + 2], k, h)
 
     def terms(step):
         for k in range(half):
             tokens[step].gather_term(hidden, held[3 * step + 2], own, k)
 
-    def reduce(step, k):
-        for c in range(CHUNKS):
+    def reduce(step, k, h):
+        for c in chunks_of(h):
             tokens[step].reduce(own, k, c)
 
     def hand_back():
@@ -406,42 +413,54 @@
     moves.send(3, 1)
     moves.send(3, 2)
     moves.send(3, 3)
+    moves.send(4, 0)
+    moves.send(4, 1)
+    moves.send(4, 2)
+    moves.send(4, 3)
     moves.relay_near(2, 3)
     moves.relay_far(1, 0)
     moves.relay_far(1, 1)
     moves.relay_far(1, 2)
     moves.relay_far(1, 3)
     start.wait()
-    tokens[0].collect()
+    collect(0, 0)
+    collect(0, 1)
     moves.settle(0)
     moves.settle(1)
-    activate(0)
-    moves.send(4, 0)
-    moves.send(4, 1)
-    moves.send(4, 2)
-    moves.send(4, 3)
+    moves.send(5, 0)
+    moves.send(5, 1)
+    moves.send(5, 2)
+    moves.send(5, 3)
+    activate(0, 0)
+    activate(0, 1)
     moves.relay_far(2, 0)
     moves.relay_far(2, 1)
     moves.relay_far(2, 2)
     moves.relay_far(2, 3)
     moves.settle(2)
-    swap(0)
+    swap(0, 0, 0)
+    swap(0, 0, 1)
+    swap(0, 1, 0)
+    swap(0, 1, 1)
+    swap(0, 2, 0)
+    swap(0, 2, 1)
+    swap(0, 3, 0)
+    swap(0, 3, 1)
     terms(0)
-    moves.send(5, 0)
-    moves.send(5, 1)
-    moves.send(5, 2)
-    moves.send(5, 3)
     moves.relay_near(3, 0)
     moves.relay_near(3, 1)
     moves.relay_near(3, 2)
     moves.relay_near(3, 3)
-    reduce(0, 0)
-    reduce(0, 1)
+    reduce(0, 0, 0)
+    reduce(0, 0, 1)
+    reduce(0, 1, 0)
+    reduce(0, 1, 1)
     moves.relay_near(4, 0)
     moves.relay_near(4, 1)
     moves.relay_near(4, 2)
     moves.relay_near(4, 3)
-    reduce(0, 2)
+    reduce(0, 2, 0)
+    reduce(0, 2, 1)
     hand_back()
     moves.relay_far(3, 0)
     moves.relay_far(3, 1)
@@ -462,16 +481,28 @@
     moves.relay_far(5, 2)
     moves.relay_far(5, 3)
     pass_on(1, 2)
-    tokens[1].collect()
+    collect(1, 0)
     moves.settle(3)
     moves.settle(4)
-    activate(1)
+    activate(1, 0)
     moves.settle(5)
-    swap(1)
+    swap(1, 0, 0)
+    collect(1, 1)
+    activate(1, 1)
+    swap(1, 0, 1)
+    swap(1, 1, 0)
+    swap(1, 1, 1)
+    swap(1, 2, 0)
+    swap(1, 2, 1)
+    swap(1, 3, 0)
+    swap(1, 3, 1)
     terms(1)
-    reduce(1, 0)
-    reduce(1, 1)
-    reduce(1, 2)
+    reduce(1, 0, 0)
+    reduce(1, 0, 1)
+    reduce(1, 1, 0)
+    reduce(1, 1, 1)
+    reduce(1, 2, 0)
+    reduce(1, 2, 1)
     deliver()
     for m in range(6):
         moves.drain(m)
@@ -642,7 +673,7 @@
     units = shape[1] * lax.axis_size("tp")
     whole_rows = shape[0] == LANES and shape[1] % LANES == 0 and units % (16 * shards) == 0
     whole_tokens = token_shape[0] % (32 * CHUNKS) == 0 and token_shape[1] % LANES == 0
-    pairs = shards % 4 == 0 and lax.axis_size("gr") == 2 and lax.axis_size("tp") == 2
+    pairs = shards == 2 * PLACES and lax.axis_size("gr") == 2 and lax.axis_size("tp") == 2
     return whole_rows and whole_tokens and pairs
 
 

time: 188 us -> 187 us (level)
  Pallas kernels: 188 us -> 186 us
where the time goes in v3:
time: 187 us
  Pallas kernels  186 us (99%)
    pallas_call x1, Pallas kernels, whole(): pl.pallas_call(functools.partial(whole_kernel, shards, features, units),...  180 us
    pallas_call x1, Pallas kernels, write_out(): pl.pallas_call(functools.partial(write_kernel, count), out_shape=[jax.Sha...  6.23 us

profile of v3, /device:TPU:0, one launch (start us, length us, event | category | flops | bytes accessed | tf_op | source)
XLA Modules:
  0.0 187.2 jit_solution(1209333784944311493)
XLA Ops:
  0.6 180.1 %shard_map.144 = (bf16[512,256]{1,0:T(8,128)(2,1)S(1)}, bf16[704,2048]{1,0:T(8,128)(2,1)S(1)}, bf16[704,2048]{1,0:T(8,128)(2,1)S(1)}, bf16[704,2048]{1,0:T(8,128...) custom-call(bf16[512,256]{1,0:T(8,128)(2,1)} %refs_0_.1, ...), custom_call_target="tpu_custom_call" | custom-call | tf_op jit(solution)/shard_map/pallas_call | solution.py:542
  180.8 6.2 %shard_map.145 = (bf16[512,256]{1,0:T(8,128)(2,1)}, bf16[704,2048]{1,0:T(8,128)(2,1)}, bf16[704,2048]{1,0:T(8,128)(2,1)}, bf16[704,2048]{1,0:T(8,128)(2,1)}, bf1...) custom-call(bf16[512,256]{1,0:T(8,128)(2,1)S(1)} %get-tuple-element.14.refs_0_, ...), custom_call_target="tpu_custom_call" | custom-call | tf_op jit(solution)/shard_map/pallas_call | solution.py:524
